TPU v7x, 32 devices: a whole 2x2x4 slice. The times are simulated.
32 devices in a mesh: sp: 8 (over z, y), tp: 4 (over x, core).
Axes of the slice: x: 2, y: 2, z: 4, core: 2. Of those that a mesh axis runs over, the one named last changes fastest.
Arguments:
- resid: bfloat16 [2048, 2048], P(('sp', 'tp')), may hold values from -6 to 6
- query_a: bfloat16 [2048, 4, 128], P('sp', 'tp')
- key_a: bfloat16 [2048, 4, 128], P('sp', 'tp')
- value_a: bfloat16 [2048, 4, 128], P('sp', 'tp'), may hold values from -6 to 6
- query_b: bfloat16 [2048, 4, 256], P('sp', 'tp')
- key_b: bfloat16 [2048, 4, 256], P('sp', 'tp')
- value_b: bfloat16 [2048, 4, 128], P('sp', 'tp'), may hold values from -6 to 6
- lambda_a: float32 [4], P('tp'), may hold values from 0.3 to 0.8
- lambda_b: float32 [4], P('tp'), may hold values from 0.3 to 0.8
- head_gain: float32 [128], replicated, may hold values from 0.1 to 1.9
- out_weight: bfloat16 [1024, 2048], replicated, may hold values from -0.1875 to 0.1875
- norm_gain: float32 [2048], replicated, may hold values from 0.1 to 1.9
- expert_ids: int32 [2048, 4], P(('sp', 'tp')), may hold values from 0 to 31, all different within a row; in each aligned block of 64 rows (0 to 63, 64 to 127, ...) at most 16 rows name the same one
- expert_mix: float32 [2048, 4], P(('sp', 'tp')), may hold values from 0.2 to 1
- gate_experts: bfloat16 [32, 2048, 1024], P(('sp', 'tp')), may hold values from -0.125 to 0.125
- up_experts: bfloat16 [32, 2048, 1024], P(('sp', 'tp')), may hold values from -0.125 to 0.125
- down_experts: bfloat16 [32, 1024, 2048], P(('sp', 'tp')), may hold values from -0.1875 to 0.1875
- shared_gate: bfloat16 [2048, 512], replicated, may hold values from -0.125 to 0.125
- shared_up: bfloat16 [2048, 512], replicated, may hold values from -0.125 to 0.125
- shared_down: bfloat16 [512, 2048], replicated, may hold values from -0.25 to 0.25
Outputs:
- layer_out: bfloat16 [2048, 2048], P(('sp', 'tp'))
Inputs may be any that keep to these rules, and one draw needn't show every extreme that they name: `expert_ids`: in each aligned block of 64 rows (the rows of one device) no expert is named more than 16 times, a bound that some block reaches.
All inputs are finite; a program needn't handle non-finite values.
Results may differ from a plain program's by a relative error of at most 0.017.
Values may be sent and summed in bfloat16 or wider, within the bound.
No kernel may reach another device: no remote copies, remote signals or barrier semaphores. Data moves between devices by JAX's collectives and lax.ppermute only.
A program may use at most 128 MiB of HBM per device.

v0:
```python
import math
import jax
import jax.numpy as jnp
from jax import lax
from jax.sharding import PartitionSpec as P

NEG_FILL = -1e30
EPSILON = 1e-05
HEAD_SCALE = 0.8
KEY_SPAN = 2048


def swiglu_rows(row_set, w_gate, w_up, w_down):
    gate_val = jnp.dot(row_set, w_gate, preferred_element_type=jnp.float32)
    up_val = jnp.dot(row_set, w_up, preferred_element_type=jnp.float32)
    hidden = (jax.nn.silu(gate_val) * up_val).astype(jnp.bfloat16)
    return jnp.dot(hidden, w_down, preferred_element_type=jnp.float32)


def online_update(state, query_map, key_map, value_block, causal, scaling):
    row_top, denoms, numerator = state
    scores = (
        jnp.einsum("qhd,khd->hqk", query_map, key_map, preferred_element_type=jnp.float32) * scaling
    )
    scores = jnp.where(causal, scores, NEG_FILL)
    new_top = jnp.maximum(row_top, jnp.max(scores, axis=2))
    exponent = jnp.where(causal, jnp.exp(scores - new_top[:, :, None]), 0.0)
    shrink = jnp.exp(row_top - new_top)
    denoms = denoms * shrink + jnp.sum(exponent, axis=2)
    numerator = numerator * jnp.transpose(shrink)[:, :, None] + jnp.einsum(
        "hqk,khe->qhe",
        exponent.astype(jnp.bfloat16),
        value_block,
        preferred_element_type=jnp.float32,
    )
    return (new_top, denoms, numerator)


def group_update(states, queries, key_block, value_block, causal):
    map_width = queries.shape[2] // 2
    scaling = map_width ** (-0.5)
    first_state = online_update(
        states[0],
        queries[:, :, :map_width],
        key_block[:, :, :map_width],
        value_block,
        causal,
        scaling,
    )
    second_state = online_update(
        states[1],
        queries[:, :, map_width:],
        key_block[:, :, map_width:],
        value_block,
        causal,
        scaling,
    )
    return (first_state, second_state)


def empty_state(query_rows, head_count, value_width):
    single = (
        jnp.full((head_count, query_rows), NEG_FILL, jnp.float32),
        jnp.zeros((head_count, query_rows), jnp.float32),
        jnp.zeros((query_rows, head_count, value_width), jnp.float32),
    )
    return (single, single)


def finish_group(states, lambdas, head_gain):
    first_out = states[0][2] / jnp.transpose(states[0][1])[:, :, None]
    second_out = states[1][2] / jnp.transpose(states[1][1])[:, :, None]
    differ = first_out - lambdas[None, :, None] * second_out
    scale_rms = lax.rsqrt(jnp.mean(differ * differ, axis=2, keepdims=True) + EPSILON)
    return (differ * scale_rms * head_gain[None, None, :] * HEAD_SCALE).astype(jnp.bfloat16)


def per_device(
    resid,
    query_a,
    key_a,
    value_a,
    query_b,
    key_b,
    value_b,
    lambda_a,
    lambda_b,
    head_gain,
    out_weight,
    norm_gain,
    expert_ids,
    expert_mix,
    gate_experts,
    up_experts,
    down_experts,
    shared_gate,
    shared_up,
    shared_down,
):
    query_rows = query_a.shape[0]
    value_width = value_a.shape[2]
    query_pos = lax.axis_index("sp") * query_rows + jnp.arange(query_rows, dtype=jnp.int32)
    start_state = (
        empty_state(query_rows, query_a.shape[1], value_width),
        empty_state(query_rows, query_b.shape[1], value_width),
    )
    key_piece_a = lax.all_gather(key_a, "sp", axis=0, tiled=True)
    value_piece_a = lax.all_gather(value_a, "sp", axis=0, tiled=True)
    key_piece_b = lax.all_gather(key_b, "sp", axis=0, tiled=True)
    value_piece_b = lax.all_gather(value_b, "sp", axis=0, tiled=True)
    piece_rows = key_piece_a.shape[0]
    step_rows = math.gcd(piece_rows, KEY_SPAN)

    def one_step(step_index, inner_state):
        begin_row = step_index * step_rows
        key_pos = begin_row + jnp.arange(step_rows, dtype=jnp.int32)
        causal = (key_pos[None, :] <= query_pos[:, None])[None]
        part_a = group_update(
            inner_state[0],
            query_a,
            lax.dynamic_slice_in_dim(key_piece_a, begin_row, step_rows, 0),
            lax.dynamic_slice_in_dim(value_piece_a, begin_row, step_rows, 0),
            causal,
        )
        part_b = group_update(
            inner_state[1],
            query_b,
            lax.dynamic_slice_in_dim(key_piece_b, begin_row, step_rows, 0),
            lax.dynamic_slice_in_dim(value_piece_b, begin_row, step_rows, 0),
            causal,
        )
        return (part_a, part_b)

    state_a, state_b = lax.fori_loop(0, piece_rows // step_rows, one_step, start_state)
    heads_a = finish_group(state_a, lambda_a, head_gain)
    heads_b = finish_group(state_b, lambda_b, head_gain)
    tok_dev = resid.shape[0]
    back_a, back_b = (
        lax.all_to_all(heads_a, "tp", split_axis=0, concat_axis=1, tiled=True),
        lax.all_to_all(heads_b, "tp", split_axis=0, concat_axis=1, tiled=True),
    )
    joined = jnp.concatenate([back_a.reshape(tok_dev, -1), back_b.reshape(tok_dev, -1)], axis=1)
    project = jnp.dot(joined, out_weight, preferred_element_type=jnp.float32)
    middle = (resid.astype(jnp.float32) + project).astype(jnp.bfloat16)
    middle_f = middle.astype(jnp.float32)
    normed = (
        middle_f
        * lax.rsqrt(jnp.mean(middle_f * middle_f, axis=1, keepdims=True) + EPSILON)
        * norm_gain[None, :]
    ).astype(jnp.bfloat16)
    shared = swiglu_rows(normed, shared_gate, shared_up, shared_down)
    top_count = expert_ids.shape[1]
    model_width = normed.shape[1]
    sp_count = lax.axis_size("sp")
    tp_count = lax.axis_size("tp")
    expert_total = sp_count * tp_count
    pair_count = tok_dev * top_count
    capacity = max(2, 2 * pair_count // expert_total)
    flat_ids = expert_ids.reshape(-1)
    one_hot = (flat_ids[:, None] == jnp.arange(expert_total, dtype=jnp.int32)[None, :]).astype(
        jnp.int32
    )
    pair_rank = jnp.sum((jnp.cumsum(one_hot, axis=0) - one_hot) * one_hot, axis=1)
    pair_token = jnp.arange(pair_count, dtype=jnp.int32) // top_count
    send_rows = (
        jnp.zeros((expert_total, capacity, model_width), jnp.bfloat16)
        .at[flat_ids, pair_rank]
        .set(normed[pair_token])
    )
    arrived = lax.all_to_all(send_rows, ("sp", "tp"), split_axis=0, concat_axis=0, tiled=True)
    arrived_shape = arrived.shape
    flat_rows = arrived.reshape(-1, arrived_shape[-1])
    result = swiglu_rows(flat_rows, gate_experts[0], up_experts[0], down_experts[0]).astype(
        jnp.bfloat16
    )
    finished = result.reshape(arrived_shape)
    returned = lax.all_to_all(finished, ("sp", "tp"), split_axis=0, concat_axis=0, tiled=True)
    chosen = returned[flat_ids, pair_rank].reshape(tok_dev, top_count, model_width)
    routed = jnp.sum(chosen.astype(jnp.float32) * expert_mix[:, :, None], axis=1)
    return (middle_f + shared + routed).astype(jnp.bfloat16)


def solution(mesh):
    in_specs = (
        P(("sp", "tp"), None),
        P("sp", "tp", None),
        P("sp", "tp", None),
        P("sp", "tp", None),
        P("sp", "tp", None),
        P("sp", "tp", None),
        P("sp", "tp", None),
        P("tp"),
        P("tp"),
        P(),
        P(),
        P(),
        P(("sp", "tp"), None),
        P(("sp", "tp"), None),
        P(("sp", "tp"), None, None),
        P(("sp", "tp"), None, None),
        P(("sp", "tp"), None, None),
        P(),
        P(),
        P(),
    )
    out_specs = P(("sp", "tp"), None)
    return jax.shard_map(
        per_device, mesh=mesh, in_specs=in_specs, out_specs=out_specs, check_vma=False
    )
```

profile of v0, /device:TPU:0, one launch (start us, length us, event | category | flops | bytes accessed | tf_op | source)
XLA Modules:
  0.0 333.9 jit_solution(18437636033774966400)
XLA Ops:
  7.3 33.6 %all_gather.12 = bf16[2048,1,128]{2,0,1:T(8,128)(2,1)S(1)} all-gather(bf16[256,1,128]{2,0,1:T(8,128)(2,1)} %param.22), channel_id=1, replica_groups=mesh['sp'=8,'tp'=4] {'sp'}, dimensions={0}, use_global_device_ids=true | all-gather | bytes 589824 | tf_op jit(solution)/shard_map/all_gather | solution.py:107
  44.2 2.8 fusion.88
  47.0 1.8 fusion.89
  48.9 31.4 %all_gather.15 = bf16[2048,1,128]{2,0,1:T(8,128)(2,1)S(1)} all-gather(bf16[256,1,128]{2,0,1:T(8,128)(2,1)S(1)} %copy-done.5), channel_id=1, replica_groups=mesh['sp'=8,'tp'=4] {'sp'}, dimensions={0}, use_global_device_ids=true | all-gather | bytes 589824 | tf_op jit(solution)/shard_map/all_gather | solution.py:110
  80.3 31.5 %all_gather.13 = bf16[2048,1,128]{2,0,1:T(8,128)(2,1)S(1)} all-gather(bf16[256,1,128]{2,0,1:T(8,128)(2,1)S(1)} %copy-done.6), channel_id=1, replica_groups=mesh['sp'=8,'tp'=4] {'sp'}, dimensions={0}, use_global_device_ids=true | all-gather | bytes 589824 | tf_op jit(solution)/shard_map/all_gather | solution.py:108
  111.8 1.8 fusion.91
  115.4 2.1 fusion.19
  122.5 3.3 all-to-all-start.1
  127.3 2.6 all-to-all-done.1
  129.9 3.3 all-to-all-start
  133.3 3.9 %all-to-all-done = bf16[4,2,4096]{2,1,0:T(2,128)(2,1)S(1)} async-done(((bf16[4,2,4096]{2,1,0:T(2,128)(2,1)}), bf16[4,2,4096]{2,1,0:T(2,128)(2,1)S(1)}, u32[]{:S(2)}, u32[]{:S(2)}) %all-to-all-start) | async-done | bytes 65568 | tf_op jit(solution)/shard_map/all_to_all | solution.py:139
  137.4 3.2 multiply_reduce_fusion.1
  140.7 2.3 gather_fusion
  144.7 46.2 %scatter_fusion = bf16[32,16,2048]{2,1,0:T(8,128)(2,1)} fusion(bf16[32,16,2048]{2,1,0:T(8,128)(2,1)} %broadcast_in_dim.49, s32[256]{0:T(256)S(1)} %bitcast.169, bf16[256,2048]{1,0:T(8,128)(2,1)} %gather_fusion), kind=kCustom, calls=%fused_computation.2 | custom fusion | bytes 3147776 | tf_op jit(solution)/shard_map/scatter | solution.py:168
  190.9 53.7 %all_to_all.40 = bf16[32,16,2048]{2,1,0:T(8,128)(2,1)S(1)} all-to-all(bf16[32,16,2048]{2,1,0:T(8,128)(2,1)} %scatter_fusion), channel_id=1, replica_groups=mesh['sp'=8,'tp'=4] {'sp','tp'}, dimensions={0} | all-to-all | bytes 4194304 | tf_op jit(solution)/shard_map/all_to_all | solution.py:170
  246.0 3.6 %fusion.4 = f32[512,1024]{1,0:T(8,128)} fusion(bf16[512,2048]{1,0:T(8,128)(2,1)S(1)} %bitcast.171, bf16[1,2048,1024]{2,1,0:T(8,128)(2,1)S(1)} %copy-done.10), kind=kOutput, calls=%fused_computation.7 | convolution fusion | flops 2147483648 | bytes 8388608 | tf_op jit(solution)/shard_map/dot_general | solution.py:14
  249.6 10.6 %fusion.6 = bf16[512,2048]{1,0:T(8,128)(2,1)} fusion(bf16[1,1024,2048]{2,1,0:T(8,128)(2,1)} %param.36, f32[512,1024]{1,0:T(8,128)} %fusion.4, bf16[512,2048]{1,0:T(8,128)(2,1)} %bitcast.172, bf16[1,2048,1024]{2,1,0:T(8,128)(2,1)} %param.35), kind=kOutput, calls=%fused_computation.9 | convolution fusion | flops 4299161600 | bytes 14680064 | tf_op jit(solution)/shard_map/dot_general | solution.py:17
  260.2 3.8 %all-to-all-start.3 = ((bf16[32,16,2048]{2,1,0:T(8,128)(2,1)}), bf16[32,16,2048]{2,1,0:T(8,128)(2,1)}, u32[]{:S(2)}, u32[]{:S(2)}) async-start(bf16[32,16,2048]{2,1,0:T(8,128)(2,1)} %bitcast.170), calls=%async_computation.3 | async-start | bytes 4194304 | tf_op jit(solution)/shard_map/all_to_all | solution.py:177
  264.7 2.1 fusion.92
  266.8 45.9 %all-to-all-done.3 = bf16[32,16,2048]{2,1,0:T(8,128)(2,1)} async-done(((bf16[32,16,2048]{2,1,0:T(8,128)(2,1)}), bf16[32,16,2048]{2,1,0:T(8,128)(2,1)}, u32[]{:S(2)}, u32[]{:S(2)}) %all-to-all-start.3) | async-done | bytes 2097184 | tf_op jit(solution)/shard_map/all_to_all | solution.py:177
  312.7 5.1 %gather_fusion.1 = bf16[256,2048]{1,0:T(8,128)(2,1)} fusion(bf16[32,16,2048]{2,1,0:T(8,128)(2,1)} %all-to-all-done.3, s32[256]{0:T(256)S(1)} %bitcast.168), kind=kCustom, calls=%fused_computation.1 | custom fusion | bytes 2099200 | tf_op jit(solution)/shard_map/gather | solution.py:178
  317.9 2.7 reshape.410
  320.6 3.2 multiply_reduce_fusion
  323.8 3.2 fusion.14
  (76 shorter events, 15.0 us)
Async XLA Ops:
  6.5 317.3 %copy-start = (bf16[512,2048]{1,0:T(8,128)(2,1)S(1)}, bf16[512,2048]{1,0:T(8,128)(2,1)}, u32[]{:S(2)}) copy-start(bf16[512,2048]{1,0:T(8,128)(2,1)} %param.39) | copy-start | bytes 6291460
  6.5 40.5 %copy-start.12 = (bf16[256,1,128]{2,0,1:T(8,128)(2,1)S(1)}, bf16[256,1,128]{2,0,1:T(8,128)(2,1)}, u32[]{:S(2)}) copy-start(bf16[256,1,128]{2,0,1:T(8,128)(2,1)} %param.21) | copy-start | bytes 196612
  6.5 105.2 %all-gather.2.cloned.1.call-start = ((), (), s32[]{:S(2)}) async-start(), calls=%async_computation.4 | async-start | bytes 1179648 | tf_op jit(solution)/shard_map/all_gather | solution.py:109
  47.0 1.9 copy-start.5
  47.0 33.3 %copy-start.6 = (bf16[256,1,128]{2,0,1:T(8,128)(2,1)S(1)}, bf16[256,1,128]{2,0,1:T(8,128)(2,1)}, u32[]{:S(2)}) copy-start(bf16[256,1,128]{2,0,1:T(8,128)(2,1)} %param.23) | copy-start | bytes 196612
  47.0 64.8 %copy-start.11 = (bf16[256,1,256]{2,0,1:T(8,128)(2,1)S(1)}, bf16[256,1,256]{2,0,1:T(8,128)(2,1)}, u32[]{:S(2)}) copy-start(bf16[256,1,256]{2,0,1:T(8,128)(2,1)} %param.24) | copy-start | bytes 393220
  111.8 3.6 %copy-start.2 = (f32[256,2048]{1,0:T(8,128)S(1)}, f32[256,2048]{1,0:T(8,128)}, u32[]{:S(2)}) copy-start(f32[256,2048]{1,0:T(8,128)} %get-tuple-element.62) | copy-start | bytes 6291460
  113.6 1.8 copy-start.1
  119.6 0.7 copy-start.9
  120.3 17.1 %copy-start.4 = (bf16[64,2048]{1,0:T(8,128)(2,1)S(1)}, bf16[64,2048]{1,0:T(8,128)(2,1)}, u32[]{:S(2)}) copy-start(bf16[64,2048]{1,0:T(8,128)(2,1)} %param.20) | copy-start | bytes 786436
  122.5 7.4 %all-to-all-start.1 = ((bf16[4,2,4096]{2,1,0:T(2,128)(2,1)}), bf16[4,2,4096]{2,1,0:T(2,128)(2,1)S(1)}, u32[]{:S(2)}, u32[]{:S(2)}) async-start(bf16[4,2,4096]{2,1,0:T(2,128)(2,1)} %reshape.432), calls=%async_computation.1 | async-start | bytes 131072 | tf_op jit(solution)/shard_map/all_to_all | solution.py:140
  129.9 7.4 %all-to-all-start = ((bf16[4,2,4096]{2,1,0:T(2,128)(2,1)}), bf16[4,2,4096]{2,1,0:T(2,128)(2,1)S(1)}, u32[]{:S(2)}, u32[]{:S(2)}) async-start(bf16[4,2,4096]{2,1,0:T(2,128)(2,1)} %reshape.434), calls=%async_computation | async-start | bytes 131072 | tf_op jit(solution)/shard_map/all_to_all | solution.py:139
  137.4 3.2 copy-start.7
  190.9 55.0 %copy-start.10 = (bf16[1,2048,1024]{2,1,0:T(8,128)(2,1)S(1)}, bf16[1,2048,1024]{2,1,0:T(8,128)(2,1)}, u32[]{:S(2)}) copy-start(bf16[1,2048,1024]{2,1,0:T(8,128)(2,1)} %param.34) | copy-start | bytes 12582916
  244.6 1.3 copy-start.3
  260.2 3.8 %copy-start.8 = (f32[64,4]{0,1:T(4,128)S(1)}, f32[64,4]{0,1:T(4,128)}, u32[]{:S(2)}) copy-start(f32[64,4]{0,1:T(4,128)} %param.33) | copy-start | bytes 3076
  260.2 52.5 %all-to-all-start.3 = ((bf16[32,16,2048]{2,1,0:T(8,128)(2,1)}), bf16[32,16,2048]{2,1,0:T(8,128)(2,1)}, u32[]{:S(2)}, u32[]{:S(2)}) async-start(bf16[32,16,2048]{2,1,0:T(8,128)(2,1)} %bitcast.170), calls=%async_computation.3 | async-start | bytes 4194304 | tf_op jit(solution)/shard_map/all_to_all | solution.py:177
Sparse Core Ops, SparseCore 0:
  9.5 43.6 all-gather.1
where the time goes:
time: 336 us; the launch traced here: 334 us
  blocking collectives  150 us (45%)
  local copies, waits for them, and re-layouts  63.9 us (19%)
  waiting for transfers between devices  53.1 us (16%)
  matrix products  33.6 us (10%)
  between operations  15.1 us (4%)
  starting transfers between devices  10.4 us (3%)
  other arithmetic  7.7 us (2%)
    all_to_all x1, blocking collectives, per_device(): lax.all_to_all(send_rows, ('sp', 'tp'), split_axis=0, concat_axis=0, tile...  53.7 us
    scatter x1, local copies, waits for them, and re-layouts, per_device(): send_rows = jnp.zeros((expert_total, capacity, model_width), jnp.bfloat16...  46.2 us
    all_to_all x1, waiting for transfers between devices, per_device(): lax.all_to_all(finished, ('sp', 'tp'), split_axis=0, concat_axis=0, tiled...  45.9 us
    all_gather x1, blocking collectives, per_device(): key_piece_a = lax.all_gather(key_a, 'sp', axis=0, tiled=True)  33.6 us
    all_gather x1, blocking collectives, per_device(): value_piece_a = lax.all_gather(value_a, 'sp', axis=0, tiled=True)  31.5 us
    all_gather x1, blocking collectives, per_device(): value_piece_b = lax.all_gather(value_b, 'sp', axis=0, tiled=True)  31.4 us
    dot_general x2, matrix products, swiglu_rows(): return jnp.dot(hidden, w_down, preferred_element_type=jnp.float32)  13.8 us
    dot_general x4, matrix products, online_update(): jnp.einsum('qhd,khd->hqk', query_map, key_map, preferred_element_type=jnp...  8.17 us
  transfers between devices with their start and end apart: 4, of which 3 were waited for; matrix products, arithmetic and copies ran while one was open for 3% of the time, Pallas kernels for 0%

commit v1 on v0

--- a/solution.py
+++ b/solution.py
@@ -3,6 +3,7 @@
 import jax.numpy as jnp
 from jax import lax
 from jax.sharding import PartitionSpec as P
+from jax.lax import axis_index, axis_size, ppermute
 
 NEG_FILL = -1e30
 EPSILON = 1e-05
@@ -104,7 +105,16 @@
         empty_state(query_rows, query_a.shape[1], value_width),
         empty_state(query_rows, query_b.shape[1], value_width),
     )
-    key_piece_a = lax.all_gather(key_a, "sp", axis=0, tiled=True)
+    n_lanes = axis_size("sp")
+    reached = key_a
+    series = [reached]
+    ready = sorted(((t, (t + 1) % n_lanes) for t in range(n_lanes)))
+    for j0 in range(1, n_lanes):
+        reached = ppermute(reached, axis_name="sp", perm=ready)
+        series.insert(0, reached)
+    key_piece_a = jnp.roll(
+        jnp.concatenate(series, axis=0), (axis_index("sp") + 1) * key_a.shape[0], axis=0
+    )
     value_piece_a = lax.all_gather(value_a, "sp", axis=0, tiled=True)
     key_piece_b = lax.all_gather(key_b, "sp", axis=0, tiled=True)
     value_piece_b = lax.all_gather(value_b, "sp", axis=0, tiled=True)

time: 336 us -> 340 us (1.012)
  blocking collectives: 150 us -> 116 us
  waiting for transfers between devices: 53.1 us -> 84.5 us
  starting transfers between devices: 10.4 us -> 15.3 us
  local copies, waits for them, and re-layouts: 63.9 us -> 67.4 us
    all_gather x1 -> x0, blocking collectives: 33.6 us -> none  [per_device(): key_piece_a = lax.all_gather(key_a, 'sp', axis=0, tiled=True)]
    ppermute x0 -> x7, waiting for transfers between devices: none -> 32.1 us  [per_device(): reached = ppermute(reached, axis_name='sp', perm=ready)]
    ppermute x0 -> x7, starting transfers between devices: none -> 5.04 us  [per_device(): reached = ppermute(reached, axis_name='sp', perm=ready)]
    unnamed x38 -> x51, local copies, waits for them, and re-layouts: 4.57 us -> 8.14 us
  transfers between devices with their start and end apart: 4 -> 11, of which waited for: 3 -> 8; matrix products, arithmetic and copies ran while one was open for 3% -> 4% of each run, Pallas kernels for 0% -> 0%
where the time goes in v1:
time: 340 us; the launch traced here: 338 us
  blocking collectives  116 us (34%)
  waiting for transfers between devices  84.5 us (25%)
  local copies, waits for them, and re-layouts  67.4 us (20%)
  matrix products  32.2 us (9%)
  starting transfers between devices  15.3 us (4%)
  between operations  15.1 us (4%)
  other arithmetic  7.12 us (2%)
    all_to_all x1, blocking collectives, per_device(): lax.all_to_all(send_rows, ('sp', 'tp'), split_axis=0, concat_axis=0, tile...  51.9 us
    scatter x1, local copies, waits for them, and re-layouts, per_device(): send_rows = jnp.zeros((expert_total, capacity, model_width), jnp.bfloat16...  46.2 us
    all_to_all x1, waiting for transfers between devices, per_device(): lax.all_to_all(finished, ('sp', 'tp'), split_axis=0, concat_axis=0, tiled...  45.9 us
    all_gather x1, blocking collectives, per_device(): value_piece_b = lax.all_gather(value_b, 'sp', axis=0, tiled=True)  32.2 us
    ppermute x7, waiting for transfers between devices, per_device(): reached = ppermute(reached, axis_name='sp', perm=ready)  32.1 us
    all_gather x1, blocking collectives, per_device(): value_piece_a = lax.all_gather(value_a, 'sp', axis=0, tiled=True)  31.8 us
    dot_general x2, matrix products, swiglu_rows(): return jnp.dot(hidden, w_down, preferred_element_type=jnp.float32)  13.8 us
    unnamed x51, local copies, waits for them, and re-layouts  8.14 us
  transfers between devices with their start and end apart: 11, of which 8 were waited for; matrix products, arithmetic and copies ran while one was open for 4% of the time, Pallas kernels for 0%

profile of v1, /device:TPU:0, one launch (start us, length us, event | category | flops | bytes accessed | tf_op | source)
XLA Modules:
  0.0 337.7 jit_solution(4283059583685503015)
XLA Ops:
  6.5 3.0 collective-permute-start
  9.6 32.2 %all_gather.11 = bf16[2048,1,128]{2,0,1:T(8,128)(2,1)S(1)} all-gather(bf16[256,1,128]{2,0,1:T(8,128)(2,1)} %param.26), channel_id=1, replica_groups=mesh['sp'=8,'tp'=4] {'sp'}, dimensions={0}, use_global_device_ids=true | all-gather | bytes 589824 | tf_op jit(solution)/shard_map/all_gather | solution.py:120
  42.8 31.8 %all_gather.9 = bf16[2048,1,128]{2,0,1:T(8,128)(2,1)S(1)} all-gather(bf16[256,1,128]{2,0,1:T(8,128)(2,1)} %param.23), channel_id=1, replica_groups=mesh['sp'=8,'tp'=4] {'sp'}, dimensions={0}, use_global_device_ids=true | all-gather | bytes 589824 | tf_op jit(solution)/shard_map/all_gather | solution.py:118
  77.3 5.2 %collective-permute-done.2 = bf16[256,1,128]{2,0,1:T(8,128)(2,1)S(1)} collective-permute-done((bf16[256,1,128]{2,0,1:T(8,128)(2,1)S(1)}, bf16[256,1,128]{2,0,1:T(8,128)(2,1)S(1)}, u32[]{:S(2)}, u32[]{:S(2)}) %collective-permute-start.2) | collective-permute-done | bytes 65568 | tf_op jit(solution)/shard_map/ppermute | solution.py:113
  82.8 6.7 %collective-permute-done.3 = bf16[256,1,128]{2,0,1:T(8,128)(2,1)S(1)} collective-permute-done((bf16[256,1,128]{2,0,1:T(8,128)(2,1)S(1)}, bf16[256,1,128]{2,0,1:T(8,128)(2,1)S(1)}, u32[]{:S(2)}, u32[]{:S(2)}) %collective-permute-start.3) | collective-permute-done | bytes 65568 | tf_op jit(solution)/shard_map/ppermute | solution.py:113
  89.6 7.0 %collective-permute-done.4 = bf16[256,1,128]{2,0,1:T(8,128)(2,1)} collective-permute-done((bf16[256,1,128]{2,0,1:T(8,128)(2,1)S(1)}, bf16[256,1,128]{2,0,1:T(8,128)(2,1)}, u32[]{:S(2)}, u32[]{:S(2)}) %collective-permute-start.4) | collective-permute-done | bytes 65568 | tf_op jit(solution)/shard_map/ppermute | solution.py:113
  97.9 5.9 %collective-permute-done.5 = bf16[256,1,128]{2,0,1:T(8,128)(2,1)} collective-permute-done((bf16[256,1,128]{2,0,1:T(8,128)(2,1)}, bf16[256,1,128]{2,0,1:T(8,128)(2,1)}, u32[]{:S(2)}, u32[]{:S(2)}) %collective-permute-start.5) | collective-permute-done | bytes 65568 | tf_op jit(solution)/shard_map/ppermute | solution.py:113
  103.9 7.2 %collective-permute-done.6 = bf16[256,1,128]{2,0,1:T(8,128)(2,1)S(1)} collective-permute-done((bf16[256,1,128]{2,0,1:T(8,128)(2,1)}, bf16[256,1,128]{2,0,1:T(8,128)(2,1)S(1)}, u32[]{:S(2)}, u32[]{:S(2)}) %collective-permute-start.6) | collective-permute-done | bytes 65568 | tf_op jit(solution)/shard_map/ppermute | solution.py:113
  128.1 3.3 all-to-all-start.1
  132.9 2.6 all-to-all-done.1
  135.5 3.3 all-to-all-start
  139.0 3.9 %all-to-all-done = bf16[4,2,4096]{2,1,0:T(2,128)(2,1)S(1)} async-done(((bf16[4,2,4096]{2,1,0:T(2,128)(2,1)}), bf16[4,2,4096]{2,1,0:T(2,128)(2,1)S(1)}, u32[]{:S(2)}, u32[]{:S(2)}) %all-to-all-start) | async-done | bytes 65568 | tf_op jit(solution)/shard_map/all_to_all | solution.py:149
  143.1 3.2 multiply_reduce_fusion.1
  146.4 2.3 gather_fusion
  150.3 46.2 %scatter_fusion = bf16[32,16,2048]{2,1,0:T(8,128)(2,1)} fusion(bf16[32,16,2048]{2,1,0:T(8,128)(2,1)} %broadcast_in_dim.49, s32[256]{0:T(256)S(1)} %bitcast.177, bf16[256,2048]{1,0:T(8,128)(2,1)} %gather_fusion), kind=kCustom, calls=%fused_computation.2 | custom fusion | bytes 3147776 | tf_op jit(solution)/shard_map/scatter | solution.py:178
  196.6 51.9 %all_to_all.40 = bf16[32,16,2048]{2,1,0:T(8,128)(2,1)S(1)} all-to-all(bf16[32,16,2048]{2,1,0:T(8,128)(2,1)} %scatter_fusion), channel_id=1, replica_groups=mesh['sp'=8,'tp'=4] {'sp','tp'}, dimensions={0} | all-to-all | bytes 4194304 | tf_op jit(solution)/shard_map/all_to_all | solution.py:180
  249.8 3.6 %fusion.4 = f32[512,1024]{1,0:T(8,128)} fusion(bf16[512,2048]{1,0:T(8,128)(2,1)S(1)} %bitcast.179, bf16[1,2048,1024]{2,1,0:T(8,128)(2,1)S(1)} %copy-done.9), kind=kOutput, calls=%fused_computation.7 | convolution fusion | flops 2147483648 | bytes 8388608 | tf_op jit(solution)/shard_map/dot_general | solution.py:15
  253.4 10.6 %fusion.6 = bf16[512,2048]{1,0:T(8,128)(2,1)} fusion(bf16[1,1024,2048]{2,1,0:T(8,128)(2,1)} %param.36, f32[512,1024]{1,0:T(8,128)} %fusion.4, bf16[512,2048]{1,0:T(8,128)(2,1)} %bitcast.180, bf16[1,2048,1024]{2,1,0:T(8,128)(2,1)} %param.35), kind=kOutput, calls=%fused_computation.9 | convolution fusion | flops 4299161600 | bytes 14680064 | tf_op jit(solution)/shard_map/dot_general | solution.py:18
  264.0 3.7 %all-to-all-start.3 = ((bf16[32,16,2048]{2,1,0:T(8,128)(2,1)}), bf16[32,16,2048]{2,1,0:T(8,128)(2,1)}, u32[]{:S(2)}, u32[]{:S(2)}) async-start(bf16[32,16,2048]{2,1,0:T(8,128)(2,1)} %bitcast.178), calls=%async_computation.3 | async-start | bytes 4194304 | tf_op jit(solution)/shard_map/all_to_all | solution.py:187
  270.5 45.9 %all-to-all-done.3 = bf16[32,16,2048]{2,1,0:T(8,128)(2,1)} async-done(((bf16[32,16,2048]{2,1,0:T(8,128)(2,1)}), bf16[32,16,2048]{2,1,0:T(8,128)(2,1)}, u32[]{:S(2)}, u32[]{:S(2)}) %all-to-all-start.3) | async-done | bytes 2097184 | tf_op jit(solution)/shard_map/all_to_all | solution.py:187
  316.5 5.1 %gather_fusion.1 = bf16[256,2048]{1,0:T(8,128)(2,1)} fusion(bf16[32,16,2048]{2,1,0:T(8,128)(2,1)} %all-to-all-done.3, s32[256]{0:T(256)S(1)} %bitcast.176), kind=kCustom, calls=%fused_computation.1 | custom fusion | bytes 2099200 | tf_op jit(solution)/shard_map/gather | solution.py:188
  321.6 2.7 reshape.410
  324.4 3.2 multiply_reduce_fusion
  327.6 3.2 fusion.16
  (103 shorter events, 28.6 us)
Async XLA Ops:
  6.5 321.0 %copy-start = (bf16[512,2048]{1,0:T(8,128)(2,1)S(1)}, bf16[512,2048]{1,0:T(8,128)(2,1)}, u32[]{:S(2)}) copy-start(bf16[512,2048]{1,0:T(8,128)(2,1)} %param.39) | copy-start | bytes 6291460
  6.5 106.3 %copy-start.4 = (bf16[256,1,128]{2,0,1:T(8,128)(2,1)S(1)}, bf16[256,1,128]{2,0,1:T(8,128)(2,1)}, u32[]{:S(2)}) copy-start(bf16[256,1,128]{2,0,1:T(8,128)(2,1)} %param.22) | copy-start | bytes 196612
  6.5 111.9 %all-gather.2.cloned.1.call-start = ((), (), s32[]{:S(2)}) async-start(), calls=%async_computation.4 | async-start | bytes 1179648 | tf_op jit(solution)/shard_map/all_gather | solution.py:119
  6.5 35.2 %collective-permute-start = (bf16[256,1,128]{2,0,1:T(8,128)(2,1)}, bf16[256,1,128]{2,0,1:T(8,128)(2,1)S(1)}, u32[]{:S(2)}, u32[]{:S(2)}) collective-permute-start(bf16[256,1,128]{2,0,1:T(8,128)(2,1)} %param.22), channel_id=1, source_target_pairs={{0,4},{4,8},{8,12},{12,16},{16,20},{20,24},{24,28},{28,0},{1,5},{5... | collective-permute-start | bytes 196616 | tf_op jit(solution)/shard_map/ppermute | solution.py:113
  41.8 33.8 %collective-permute-start.1 = (bf16[256,1,128]{2,0,1:T(8,128)(2,1)S(1)}, bf16[256,1,128]{2,0,1:T(8,128)(2,1)S(1)}, u32[]{:S(2)}, u32[]{:S(2)}) collective-permute-start(bf16[256,1,128]{2,0,1:T(8,128)(2,1)S(1)} %collective-permute-done), channel_id=1, source_target_pairs={{0,4},{4,8},{8,12},{12,16},{16,20},{20,24},{24,28},{28,0},{1,5},{5... | collective-permute-start | bytes 196616 | tf_op jit(solution)/shard_map/ppermute | solution.py:113
  75.5 7.0 %collective-permute-start.2 = (bf16[256,1,128]{2,0,1:T(8,128)(2,1)S(1)}, bf16[256,1,128]{2,0,1:T(8,128)(2,1)S(1)}, u32[]{:S(2)}, u32[]{:S(2)}) collective-permute-start(bf16[256,1,128]{2,0,1:T(8,128)(2,1)S(1)} %collective-permute-done.1), channel_id=1, source_target_pairs={{0,4},{4,8},{8,12},{12,16},{16,20},{20,24},{24,28},{28,0},{1,5},{5... | collective-permute-start | bytes 196616 | tf_op jit(solution)/shard_map/ppermute | solution.py:113
  82.5 7.0 %collective-permute-start.3 = (bf16[256,1,128]{2,0,1:T(8,128)(2,1)S(1)}, bf16[256,1,128]{2,0,1:T(8,128)(2,1)S(1)}, u32[]{:S(2)}, u32[]{:S(2)}) collective-permute-start(bf16[256,1,128]{2,0,1:T(8,128)(2,1)S(1)} %collective-permute-done.2), channel_id=1, source_target_pairs={{0,4},{4,8},{8,12},{12,16},{16,20},{20,24},{24,28},{28,0},{1,5},{5... | collective-permute-start | bytes 196616 | tf_op jit(solution)/shard_map/ppermute | solution.py:113
  89.5 7.1 %collective-permute-start.4 = (bf16[256,1,128]{2,0,1:T(8,128)(2,1)S(1)}, bf16[256,1,128]{2,0,1:T(8,128)(2,1)}, u32[]{:S(2)}, u32[]{:S(2)}) collective-permute-start(bf16[256,1,128]{2,0,1:T(8,128)(2,1)S(1)} %collective-permute-done.3), channel_id=1, source_target_pairs={{0,4},{4,8},{8,12},{12,16},{16,20},{20,24},{24,28},{28,0},{1,5},{5... | collective-permute-start | bytes 196616 | tf_op jit(solution)/shard_map/ppermute | solution.py:113
  96.6 7.3 %collective-permute-start.5 = (bf16[256,1,128]{2,0,1:T(8,128)(2,1)}, bf16[256,1,128]{2,0,1:T(8,128)(2,1)}, u32[]{:S(2)}, u32[]{:S(2)}) collective-permute-start(bf16[256,1,128]{2,0,1:T(8,128)(2,1)} %collective-permute-done.4), channel_id=1, source_target_pairs={{0,4},{4,8},{8,12},{12,16},{16,20},{20,24},{24,28},{28,0},{1,5},{5... | collective-permute-start | bytes 196616 | tf_op jit(solution)/shard_map/ppermute | solution.py:113
  97.9 16.8 %copy-start.11 = (bf16[256,1,128]{2,0,1:T(8,128)(2,1)S(1)}, bf16[256,1,128]{2,0,1:T(8,128)(2,1)}, u32[]{:S(2)}) copy-start(bf16[256,1,128]{2,0,1:T(8,128)(2,1)} %param.21) | copy-start | bytes 196612
  103.8 7.2 %collective-permute-start.6 = (bf16[256,1,128]{2,0,1:T(8,128)(2,1)}, bf16[256,1,128]{2,0,1:T(8,128)(2,1)S(1)}, u32[]{:S(2)}, u32[]{:S(2)}) collective-permute-start(bf16[256,1,128]{2,0,1:T(8,128)(2,1)} %collective-permute-done.5), channel_id=1, source_target_pairs={{0,4},{4,8},{8,12},{12,16},{16,20},{20,24},{24,28},{28,0},{1,5},{5... | collective-permute-start | bytes 196616 | tf_op jit(solution)/shard_map/ppermute | solution.py:113
  116.5 1.9 copy-start.10
  118.5 3.5 %copy-start.2 = (f32[256,2048]{0,1:T(8,128)S(1)}, f32[256,2048]{0,1:T(8,128)}, u32[]{:S(2)}) copy-start(f32[256,2048]{0,1:T(8,128)} %get-tuple-element.62) | copy-start | bytes 6291460
  120.2 1.8 copy-start.1
  125.3 0.7 copy-start.8
  125.9 17.1 %copy-start.5 = (bf16[64,2048]{1,0:T(8,128)(2,1)S(1)}, bf16[64,2048]{1,0:T(8,128)(2,1)}, u32[]{:S(2)}) copy-start(bf16[64,2048]{1,0:T(8,128)(2,1)} %param.20) | copy-start | bytes 786436
  128.1 7.4 %all-to-all-start.1 = ((bf16[4,2,4096]{2,1,0:T(2,128)(2,1)}), bf16[4,2,4096]{2,1,0:T(2,128)(2,1)S(1)}, u32[]{:S(2)}, u32[]{:S(2)}) async-start(bf16[4,2,4096]{2,1,0:T(2,128)(2,1)} %reshape.432), calls=%async_computation.1 | async-start | bytes 131072 | tf_op jit(solution)/shard_map/all_to_all | solution.py:150
  135.5 7.4 %all-to-all-start = ((bf16[4,2,4096]{2,1,0:T(2,128)(2,1)}), bf16[4,2,4096]{2,1,0:T(2,128)(2,1)S(1)}, u32[]{:S(2)}, u32[]{:S(2)}) async-start(bf16[4,2,4096]{2,1,0:T(2,128)(2,1)} %reshape.434), calls=%async_computation | async-start | bytes 131072 | tf_op jit(solution)/shard_map/all_to_all | solution.py:149
  143.1 3.2 copy-start.6
  196.6 53.2 %copy-start.9 = (bf16[1,2048,1024]{2,1,0:T(8,128)(2,1)S(1)}, bf16[1,2048,1024]{2,1,0:T(8,128)(2,1)}, u32[]{:S(2)}) copy-start(bf16[1,2048,1024]{2,1,0:T(8,128)(2,1)} %param.34) | copy-start | bytes 12582916
  248.5 1.3 copy-start.3
  264.0 3.7 %copy-start.7 = (f32[64,4]{0,1:T(4,128)S(1)}, f32[64,4]{0,1:T(4,128)}, u32[]{:S(2)}) copy-start(f32[64,4]{0,1:T(4,128)} %param.33) | copy-start | bytes 3076
  264.0 52.4 %all-to-all-start.3 = ((bf16[32,16,2048]{2,1,0:T(8,128)(2,1)}), bf16[32,16,2048]{2,1,0:T(8,128)(2,1)}, u32[]{:S(2)}, u32[]{:S(2)}) async-start(bf16[32,16,2048]{2,1,0:T(8,128)(2,1)} %bitcast.178), calls=%async_computation.3 | async-start | bytes 4194304 | tf_op jit(solution)/shard_map/all_to_all | solution.py:187
Sparse Core Ops, SparseCore 0:
  9.7 46.0 all-gather.1
